TPU v7x, 32 devices: a whole 2x2x4 slice. The times are simulated.
32 devices in a mesh: grp: 2 (over x), fs: 4 (over z), tp: 4 (over y, core).
Axes of the slice: x: 2, y: 2, z: 4, core: 2. Of those that a mesh axis runs over, the one named last changes fastest.
Arguments:
- tokens: bfloat16 [4096, 2048], P(('grp', 'fs')), parts along dimension 0, may hold values from -200 to 200
- norm_gain: float32 [2048], replicated, may hold values from 0.1 to 1.9
- value_weight: float32 [2048, 5632], P('fs', 'tp'), may hold values from -0.125 to 0.125
- gate_weight: float32 [2048, 5632], P('fs', 'tp'), may hold values from -0.125 to 0.125
- down_weight: float32 [2048, 5632], P('fs', 'tp'), may hold values from -0.078125 to 0.078125
- value_scale: float32 [5632], P('tp'), may hold values from 0.3 to 3
- gate_scale: float32 [5632], P('tp'), may hold values from 0.3 to 3
- down_scale: float32 [2048], replicated, may hold values from 0.3 to 3
- value_taps: float32 [3, 5632], P(None, 'tp'), may hold values from -3 to 3
- gate_taps: float32 [3, 5632], P(None, 'tp'), may hold values from -3 to 3
- value_bias: float32 [5632], P('tp'), may hold values from -3 to 3
- gate_bias: float32 [5632], P('tp'), may hold values from -3 to 3
Outputs:
- mixed: bfloat16 [4096, 2048], P(('grp', 'fs', 'tp')), parts along dimension 0
There are 2 independent parts, one for each index of `grp`. A program takes and returns all parts, laid end to end along the dimension named above; an argument that names none is the same for every part. Nothing has to cross between parts.
All inputs are finite; a program needn't handle non-finite values.
Results may differ from a plain program's by a relative error of at most 0.024.
Values may be sent and summed in bfloat16 or wider, within the bound.
A program may use at most 64 MiB of HBM per device.

v0:
```python
import functools

import jax
import jax.numpy as jnp
from jax import lax
from jax.experimental import pallas as pl
from jax.experimental.pallas import tpu as pltpu
from jax.sharding import PartitionSpec as P

MESH = pl.DeviceIdType.MESH
WIDE = 256
RIGHT, LEFT, ACROSS = 0, 1, 2


def kernel(
    parts,
    line,
    peers,
    pieces,
    lent,
    tokens,
    norm_gain,
    value_weight,
    gate_weight,
    down_weight,
    value_scale,
    gate_scale,
    down_scale,
    value_taps,
    gate_taps,
    value_bias,
    gate_bias,
    out,
    *scratch,
):
    group, here, me = lax.axis_index("grp"), lax.axis_index("fs"), lax.axis_index("tp")
    scratch = list(scratch)
    take = lambda count: [scratch.pop(0) for _ in range(count)]
    kinds = 2 if lent else 1
    full = take(3 * kinds)
    normed, partial, landed, along, wide = take(5)
    mixed, hidden = take(kinds), take(kinds)
    send_sem, recv_sem, sum_send, sum_recv = take(4)
    if lent:
        guest, guest_mixed, guest_hidden, guest_partial, guest_landed, summed, returned = take(7)
        lend_send, lend_recv, guest_send, guest_recv = take(4)
        back_send, back_recv = take(2)
    shards = (value_weight, gate_weight, down_weight)
    rows = tokens.shape[0]
    held, units = shards[0].shape
    share = held // parts
    piece = share // pieces
    kept = rows // peers
    base = (0, units - lent)
    span = (units - lent, lent)
    end = jnp.logical_or(here == 0, here == line - 1)
    inner = jnp.logical_not(end)
    helper = jnp.logical_and(inner, jnp.logical_or(here == 1, here == line - 2))
    mate = jnp.where(end, jnp.where(here == 0, 1, line - 2), jnp.where(here == 1, 0, line - 1))

    barrier = pltpu.get_barrier_semaphore()

    def greet(axis, index):
        pl.semaphore_signal(barrier, inc=1, device_id={axis: index}, device_id_type=MESH)

    pl.when(here > 0)(lambda: greet("fs", here - 1))
    pl.when(here < line - 1)(lambda: greet("fs", here + 1))
    for k in range(1, parts):
        greet("grp", lax.rem(group + k, parts))
    for k in range(1, peers):
        greet("tp", lax.rem(me + k, peers))

    def spread():
        for i, vector in enumerate((value_scale, gate_scale, value_bias, gate_bias)):
            along[i : i + 1, :] = vector[...].reshape(1, units)
        for i, vector in enumerate((norm_gain, down_scale)):
            wide[i : i + 1, :] = vector[...].reshape(1, vector.shape[0])

    def cast(which):
        step = min(held, 64)

        def body(i, carry):
            source = pl.ds(pl.multiple_of(i * step, step), step)
            target = pl.ds(pl.multiple_of(here * held + i * step, step), step)
            for kind in range(kinds):
                columns = slice(base[kind], base[kind] + span[kind])
                full[which + 3 * kind][target, :] = shards[which][source, columns].astype(
                    jnp.bfloat16
                )
            return carry

        lax.fori_loop(0, held // step, body, 0)

    def copy(which, owner, part, slot, direction, neighbour=None):
        first = pl.multiple_of(owner * held + part * share + slot * piece, piece)
        block = full[which].at[pl.ds(first, piece), :]
        if neighbour is not None:
            target = {"fs": neighbour}
        elif direction == RIGHT:
            target = {"fs": lax.min(here + 1, line - 1)}
        elif direction == LEFT:
            target = {"fs": lax.max(here - 1, 0)}
        else:
            target = {"grp": lax.rem(group + direction - ACROSS + 1, parts)}
        return pltpu.make_async_remote_copy(
            src_ref=block,
            dst_ref=block,
            send_sem=send_sem.at[which, owner, slot, direction],
            recv_sem=recv_sem.at[which, owner, part, slot],
            device_id=target,
            device_id_type=MESH,
        )

    def more(which, direction):
        edge = 0 if which < 3 else 1
        return here < line - 1 - edge if direction == RIGHT else here > edge

    def comes(which, owner):
        inside = jnp.logical_and(owner >= 0, owner < line)
        return inside if which < 3 else jnp.logical_and(inside, inner)

    def own(which, act):
        for each in range(which, 3 * kinds, 3):
            for slot in range(pieces):
                for direction in (RIGHT, LEFT):
                    pl.when(more(each, direction))(
                        lambda: act(copy(each, here, group, slot, direction))
                    )

    def direct(each):
        return bool(lent) and each != 3 * kinds - 1

    def other(which, act):
        for each in range(which, 3 * kinds, 3):
            if direct(each):
                for slot in range(pieces):
                    for k in range(1, parts):
                        part = lax.rem(group + k, parts)
                        pl.when(end)(lambda: act(copy(each, here, part, slot, ACROSS + k - 1, mate)))

    def onward(which, step, act, arrive):
        for each in range(which, 3 * kinds, 3):
            for slot in range(pieces):
                for direction in (RIGHT, LEFT):
                    owner = here - step if direction == RIGHT else here + step

                    @pl.when(comes(each, owner))
                    def _():
                        if arrive:
                            copy(each, owner, group, slot, direction).wait_recv()
                        pl.when(more(each, direction))(
                            lambda: act(copy(each, owner, group, slot, direction))
                        )

                        def share_out():
                            for k in range(parts - 1):
                                act(copy(each, owner, group, slot, ACROSS + k))

                        if step == 1 and direct(each):
                            pl.when(jnp.logical_and(owner > 0, owner < line - 1))(share_out)
                        else:
                            share_out()

    def crossed(which, step):
        for each in range(which, 3 * kinds, 3):
            for slot in range(pieces):
                for owner in (here - step, here + step):

                    @pl.when(comes(each, owner))
                    def _():
                        for k in range(parts - 1):
                            part = lax.rem(group + k + 1, parts)
                            copy(each, owner, part, slot, ACROSS + k).wait_recv()

    def start(dma):
        dma.start()

    def left(dma):
        dma.wait_send()

    def normalize(source, offset):
        step = min(rows, 64)

        def body(i, carry):
            block = pl.ds(pl.multiple_of(i * step, step), step)
            target = pl.ds(pl.multiple_of(offset + i * step, step), step)
            floated = source[block, :].astype(jnp.float32)
            mean = jnp.mean(floated * floated, axis=-1, keepdims=True)
            normed[target, :] = (floated * lax.rsqrt(mean + 1e-06) * wide[0:1, :]).astype(
                jnp.bfloat16
            )
            return carry

        lax.fori_loop(0, rows // step, body, 0)

    mine = pl.ds(pl.multiple_of(me * kept, kept), kept)

    def lend():
        return pltpu.make_async_remote_copy(
            src_ref=tokens.at[mine, :],
            dst_ref=guest.at[mine, :],
            send_sem=lend_send,
            recv_sem=lend_recv,
            device_id={"fs": mate},
            device_id_type=MESH,
        )

    def relay(k):
        return pltpu.make_async_remote_copy(
            src_ref=guest.at[mine, :],
            dst_ref=guest.at[mine, :],
            send_sem=guest_send.at[line],
            recv_sem=guest_recv.at[line],
            device_id={"tp": lax.rem(me + k, peers)},
            device_id_type=MESH,
        )

    def relays():
        lend().wait_recv()
        for k in range(1, peers):
            relay(k).start()

    def guest_rows():
        others = guest.at[pl.ds(0, (peers - 1) * kept), :]
        return others

    def welcome():
        pltpu.make_async_copy(guest_rows(), guest_rows(), guest_recv.at[line]).wait()
        normalize(guest, rows)

    def over_units(kind, body):
        count = span[kind]
        if count // WIDE:

            def one(i, carry):
                first = pl.multiple_of(i * WIDE, WIDE)
                shifted = pl.multiple_of(base[kind] + i * WIDE, 128)
                body(pl.ds(first, WIDE), pl.ds(shifted, WIDE), WIDE)
                return carry

            lax.fori_loop(0, count // WIDE, one, 0)
        if count % WIDE:
            first = count // WIDE * WIDE
            body(pl.ds(first, count % WIDE), pl.ds(base[kind] + first, count % WIDE), count % WIDE)

    def causal(which, branch, taps, offset, columns, outer, width):
        up = jnp.dot(
            normed[offset : offset + rows, :],
            full[which][:, columns],
            preferred_element_type=jnp.float32,
        )
        up = up * along[branch : branch + 1, outer]
        position = lax.broadcasted_iota(jnp.int32, (rows, width), 0)
        one = jnp.where(position >= 1, pltpu.roll(up, 1, axis=0), 0.0)
        two = jnp.where(position >= 2, pltpu.roll(up, 2, axis=0), 0.0)
        return (
            taps[0:1, outer] * two
            + taps[1:2, outer] * one
            + taps[2:3, outer] * up
            + along[branch + 2 : branch + 3, outer]
        )

    def value(kind, keep, offset):
        def body(columns, outer, width):
            keep[:, columns] = causal(
                3 * kind, 0, value_taps, offset, columns, outer, width
            )

        over_units(kind, body)

    def gate(kind, kept_value, keep, offset):
        def body(columns, outer, width):
            gated = causal(1 + 3 * kind, 1, gate_taps, offset, columns, outer, width)
            keep[:, columns] = (
                gated / (1.0 + jnp.exp(-gated)) * kept_value[:, columns]
            ).astype(jnp.bfloat16)

        over_units(kind, body)

    def give(owner, k):
        peer = lax.rem(me + k, peers)
        return pltpu.make_async_remote_copy(
            src_ref=partial.at[owner, pl.ds(pl.multiple_of(peer * kept, kept), kept), :],
            dst_ref=landed.at[k - 1, owner],
            send_sem=sum_send,
            recv_sem=sum_recv,
            device_id={"tp": peer},
            device_id_type=MESH,
        )

    def guest_give(owner, k):
        peer = lax.rem(me + k, peers)
        return pltpu.make_async_remote_copy(
            src_ref=guest_partial.at[owner, pl.ds(pl.multiple_of(peer * kept, kept), kept), :],
            dst_ref=guest_landed.at[owner, k - 1],
            send_sem=guest_send.at[owner],
            recv_sem=guest_recv.at[owner],
            device_id={"tp": peer},
            device_id_type=MESH,
        )

    def down(left_side, kind, owner):
        block = full[2 + 3 * kind][pl.ds(pl.multiple_of(owner * held, held), held), :]
        return lax.dot_general(
            left_side[...], block, (((1,), (1,)), ((), ())), preferred_element_type=jnp.float32
        )

    def project(owner):
        if not lent:
            partial[owner] = down(hidden[0], 0, owner).astype(jnp.bfloat16)
        else:

            @pl.when(helper)
            def _():
                guest_partial[owner] = down(guest_hidden, 1, owner).astype(jnp.bfloat16)
                for k in range(1, peers):
                    guest_give(owner, k).start()

            @pl.when(inner)
            def _():
                partial[owner] = (down(hidden[0], 0, owner) + down(hidden[1], 1, owner)).astype(
                    jnp.bfloat16
                )

            @pl.when(end)
            def _():
                partial[owner] = down(hidden[0], 0, owner).astype(jnp.bfloat16)

        for k in range(1, peers):
            give(owner, k).start()

    def back(owner):
        return pltpu.make_async_remote_copy(
            src_ref=summed.at[owner],
            dst_ref=returned.at[owner],
            send_sem=back_send,
            recv_sem=back_recv,
            device_id={"fs": mate},
            device_id_type=MESH,
        )

    def give_back(owner):
        if lent:

            @pl.when(helper)
            def _():
                arrived = guest_landed.at[owner]
                pltpu.make_async_copy(arrived, arrived, guest_recv.at[owner]).wait()
                total = guest_partial[owner, mine, :].astype(jnp.float32)
                for k in range(peers - 1):
                    total = total + guest_landed[owner, k].astype(jnp.float32)
                summed[owner] = total.astype(jnp.bfloat16)
                back(owner).start()

    def around(step, act):
        pl.when(here >= step)(lambda: act(here - step))
        pl.when(here + step < line)(lambda: act(here + step))

    def project_at(step):
        crossed(2, step)
        around(step, project)

    spread()
    cast(0)
    ends = (here == 0).astype(jnp.int32) + (here == line - 1).astype(jnp.int32)
    pl.semaphore_wait(barrier, parts + peers - ends)
    own(0, start)
    cast(1)
    own(1, start)
    if lent:
        pl.when(end)(lambda: lend().start())
        other(0, start)
    cast(2)
    if lent:
        pl.when(end)(lambda: own(2, start))
        other(1, start)
        other(2, start)
    normalize(tokens, 0)
    for step in range(1, line):
        onward(0, step, start, True)
        if lent and step == 1:
            pl.when(helper)(relays)
    onward(1, 1, start, True)
    if lent:
        pl.when(inner)(lambda: own(2, start))
    else:
        own(2, start)
    for step in range(1, line):
        crossed(0, step)
    value(0, mixed[0], 0)
    if lent:
        pl.when(inner)(lambda: value(1, mixed[1], 0))

        @pl.when(helper)
        def _():
            welcome()
            value(1, guest_mixed, rows)

    for step in range(2, line):
        onward(1, step, start, True)
    onward(2, 1, start, True)
    for step in range(1, line):
        crossed(1, step)
    gate(0, mixed[0], hidden[0], 0)
    if lent:
        pl.when(inner)(lambda: gate(1, mixed[1], hidden[1], 0))
        pl.when(helper)(lambda: gate(1, guest_mixed, guest_hidden, rows))
    project(here)
    for step in range(2, line):
        onward(2, step, start, True)
        project_at(step - 1)
        if step == 2:
            give_back(here)
        else:
            around(step - 2, give_back)
    project_at(line - 1)
    for step in range(max(line - 2, 1), line):
        around(step, give_back)

    pltpu.make_async_copy(landed, landed, sum_recv).wait()

    def finish(extra):
        for owner in range(line):
            total = partial[owner, mine, :].astype(jnp.float32)
            for k in range(peers - 1):
                total = total + landed[k, owner].astype(jnp.float32)
            if extra:
                total = total + returned[owner].astype(jnp.float32)
            columns = slice(owner * held, (owner + 1) * held)
            out[:, columns] = (total * wide[1:2, columns]).astype(jnp.bfloat16)

    if lent:

        @pl.when(end)
        def _():
            pltpu.make_async_copy(returned, returned, back_recv).wait()
            finish(True)
            lend().wait_send()

        pl.when(inner)(lambda: finish(False))

        @pl.when(helper)
        def _():
            pltpu.make_async_copy(guest_rows(), guest_rows(), guest_send.at[line]).wait()
            for owner in range(line):
                sent = guest_landed.at[owner]
                pltpu.make_async_copy(sent, sent, guest_send.at[owner]).wait()
            pltpu.make_async_copy(summed, summed, back_send).wait()

    else:
        finish(False)

    pltpu.make_async_copy(landed, landed, sum_send).wait()
    for which in range(3):
        own(which, left)
        other(which, left)
        for step in range(1, line):
            onward(which, step, left, False)


def solution(mesh):
    parts, line, peers = mesh.shape["grp"], mesh.shape["fs"], mesh.shape["tp"]

    def local(*arrays):
        rows, width = arrays[0].shape
        held, units = arrays[2].shape
        share = held // parts
        pieces = 2 if share % 2 == 0 and share // 2 >= 128 else 1
        kept = rows // peers
        lent = units * 5 // 11 // 128 * 128 if line >= 4 and peers > 1 else 0
        half, full = jnp.bfloat16, jnp.float32
        spans = (units - lent, lent) if lent else (units,)
        dma = pltpu.SemaphoreType.DMA
        scratch = [pltpu.VMEM((width, span), half) for span in spans for _ in range(3)]
        scratch += [
            pltpu.VMEM((rows * len(spans), width), half),
            pltpu.VMEM((line, rows, held), half),
            pltpu.VMEM((peers - 1, line, kept, held), half),
            pltpu.VMEM((4, units), full),
            pltpu.VMEM((2, width), full),
        ]
        scratch += [pltpu.VMEM((rows, span), full) for span in spans]
        scratch += [pltpu.VMEM((rows, span), half) for span in spans]
        scratch += [
            dma((3 * len(spans), line, pieces, 1 + parts)),
            dma((3 * len(spans), line, parts, pieces)),
            dma,
            dma,
        ]
        if lent:
            scratch += [
                pltpu.VMEM((rows, width), half),
                pltpu.VMEM((rows, lent), full),
                pltpu.VMEM((rows, lent), half),
                pltpu.VMEM((line, rows, held), half),
                pltpu.VMEM((line, peers - 1, kept, held), half),
                pltpu.VMEM((line, kept, held), half),
                pltpu.VMEM((line, kept, held), half),
                dma,
                dma,
                dma((line + 1,)),
                dma((line + 1,)),
                dma,
                dma,
            ]
        return pl.pallas_call(
            functools.partial(kernel, parts, line, peers, pieces, lent),
            out_shape=jax.ShapeDtypeStruct((kept, width), half),
            in_specs=[pl.BlockSpec(memory_space=pltpu.VMEM)] * 12,
            out_specs=pl.BlockSpec(memory_space=pltpu.VMEM),
            scratch_shapes=scratch,
            compiler_params=pltpu.CompilerParams(
                collective_id=0, has_side_effects=True, vmem_limit_bytes=60 * 1024 * 1024
            ),
        )(*arrays)

    return jax.shard_map(
        local,
        mesh=mesh,
        in_specs=(
            P(("grp", "fs"), None),
            P(),
            P("fs", "tp"),
            P("fs", "tp"),
            P("fs", "tp"),
            P("tp"),
            P("tp"),
            P(),
            P(None, "tp"),
            P(None, "tp"),
            P("tp"),
            P("tp"),
        ),
        out_specs=P(("grp", "fs", "tp"), None),
        check_vma=False,
    )
```

profile of v0, /device:TPU:0, one launch (start us, length us, event | category | flops | bytes accessed | tf_op | source)
XLA Modules:
  0.0 161.7 jit_solution(17029206730685741683)
XLA Ops:
  0.0 159.8 %shard_map.118 = bf16[128,2048]{1,0:T(8,128)(2,1)} custom-call(bf16[512,2048]{1,0:T(8,128)(2,1)} %tokens.1, f32[2048]{0:T(1024)} %norm_gain.1, f32[512,1408]{1,0:T(8,128)} %value_weight.1, f32[512,1408]{1,0:T(8,128)} %gate_weight.1, f32[512,1408]{1,0:T(8,128)} %down_weight.1, f32[1408]{0:T(1024)} %value_scale.1, f32[1408]{0:T(1024)} %gate_scale.1, ...), custom_call_target="tpu_custom_call" | custom-call | tf_op jit(solution)/shard_map/pallas_call | solution.py:506
  159.9 1.9 %copy.14 = bf16[128,2048]{1,0:T(8,128)(2,1)} copy(bf16[128,2048]{1,0:T(8,128)(2,1)} %shard_map.118) | data formatting | bytes 1048576
where the time goes:
time: 162 us
  Pallas kernels  160 us (99%)
  local copies, waits for them, and re-layouts  1.88 us (1%)
    pallas_call x1, Pallas kernels, local(): pl.pallas_call(functools.partial(kernel, parts, line, peers, pieces, lent...  160 us

commit v1 on v0

v1 whole, which is shorter than its diff:
```python
import functools

import jax
import jax.numpy as jnp
from jax import lax
from jax.experimental import pallas as pl
from jax.experimental.pallas import tpu as pltpu
from jax.sharding import PartitionSpec as P

MESH = pl.DeviceIdType.MESH
WIDE = 256
CUT = 2


def kernel(
    parts,
    line,
    peers,
    lent,
    tokens,
    norm_gain,
    value_weight,
    gate_weight,
    down_weight,
    value_scale,
    gate_scale,
    down_scale,
    value_taps,
    gate_taps,
    value_bias,
    gate_bias,
    out,
    *scratch,
):
    group, here, me = lax.axis_index("grp"), lax.axis_index("fs"), lax.axis_index("tp")
    scratch = list(scratch)
    take = lambda count: [scratch.pop(0) for _ in range(count)]
    kinds = 2 if lent else 1
    rows, width = tokens.shape
    held, units = value_weight.shape
    kept = rows // peers
    pairs = peers // parts
    base = (0, units - lent)
    span = (units - lent, lent)
    many = [span[k] // WIDE for k in range(kinds)]
    left_over = [span[k] % WIDE for k in range(kinds)]
    wide = [take(1)[0] if many[k] else None for k in range(kinds)]
    rest = [take(1)[0] if left_over[k] else None for k in range(kinds)]
    down = take(kinds)
    hidden = take(kinds)
    raw, normed, along, gains, partial, landed = take(6)
    send_sem, recv_sem, token_sem, along_sem, sum_send, sum_recv = take(6)
    if lent:
        guest, guest_normed, guest_hidden, guest_partial, guest_landed, summed, returned = take(7)
        guest_send, guest_recv, guest_sum_send, guest_sum_recv, back_send, back_recv = take(6)

    pair = lax.div(me, parts)
    core = lax.rem(me, parts)
    boss = core == group
    other = jnp.logical_not(boss)
    block = pair * parts + group
    sibling = pair * parts + lax.rem(core + 1, parts)
    end = jnp.logical_or(here == 0, here == line - 1)
    inner = jnp.logical_not(end)
    helper = jnp.logical_and(inner, jnp.logical_or(here == 1, here == line - 2))
    mate = jnp.where(end, jnp.where(here == 0, 1, line - 2), jnp.where(here == 1, 0, line - 1))
    both = jnp.logical_and

    barrier = pltpu.get_barrier_semaphore()

    def greet(target):
        pl.semaphore_signal(barrier, inc=1, device_id=target, device_id_type=MESH)

    pl.when(here > 0)(lambda: greet({"fs": here - 1}))
    pl.when(here < line - 1)(lambda: greet({"fs": here + 1}))
    for j in range(parts):
        for k in range(peers):
            if j or k:
                greet({"grp": lax.rem(group + j, parts), "tp": lax.rem(me + k, peers)})

    def owner_at(i):
        near = jnp.where(here < line // 2, here, line - 1 - here)
        turned = jnp.where(i % 2 == 1, near - (i + 1) // 2, near + i // 2)
        first = jnp.where(i > 2 * near, i, turned)
        return jnp.where(here < line // 2, first, line - 1 - first)

    numbers = {}
    count = 0
    for k in range(kinds):
        for name, amount in (("wide", many[k]), ("rest", 1 if left_over[k] else 0), ("down", 1)):
            numbers[name, k] = count
            count += amount * CUT

    def piece(name, kind, q, r):
        number = numbers[name, kind] + q * CUT + r

        def ref(owner):
            part = held // CUT
            first = pl.multiple_of(owner * held + r * part, part)
            if name == "wide":
                return wide[kind].at[q, :, pl.ds(first, part), :]
            if name == "rest":
                return rest[kind].at[:, pl.ds(first, part), :]
            return down[kind].at[pl.ds(first, part), :]

        return number, kind, ref

    def groups(kind, body):
        if many[kind]:

            def one(q, carry):
                body("wide", q)
                return carry

            lax.fori_loop(0, many[kind], one, 0)
        if left_over[kind]:
            body("rest", 0)

    def copy(which, owner, direction):
        number, kind, ref = which
        if direction is None:
            target, lane = {"tp": sibling}, 2
        else:
            target = {"fs": lax.clamp(0, here + direction, line - 1)}
            lane = jnp.where(direction > 0, 0, 1)
        return pltpu.make_async_remote_copy(
            src_ref=ref(owner),
            dst_ref=ref(owner),
            send_sem=send_sem.at[number, owner, lane],
            recv_sem=recv_sem.at[number, owner],
            device_id=target,
            device_id_type=MESH,
        )

    def used(kind):
        return inner if kind else here >= 0

    def further(kind, direction):
        there = here + direction
        return both(there >= kind, there <= line - 1 - kind)

    def start(dma):
        dma.start()

    def left(dma):
        dma.wait_send()

    def toward_end(direction):
        there = here + direction
        return jnp.logical_or(end, jnp.logical_or(there == 0, there == line - 1))

    def own_line(which, act, early=None):
        for direction in (1, -1):
            go = both(boss, further(which[1], direction))
            if early is True:
                go = both(go, toward_end(direction))
            elif early is False:
                go = both(go, jnp.logical_not(toward_end(direction)))
            pl.when(go)(lambda: act(copy(which, here, direction)))

    def own_across(which, act):
        pl.when(both(boss, used(which[1])))(lambda: act(copy(which, here, None)))

    def onward(which, owner, act, arrive):
        direction = jnp.where(owner < here, 1, -1)

        @pl.when(used(which[1]))
        def _():
            if arrive:
                copy(which, owner, None).wait_recv()

            @pl.when(boss)
            def _():
                pl.when(further(which[1], direction))(lambda: act(copy(which, owner, direction)))
                act(copy(which, owner, None))

    def arrive(which, owner):
        onward(which, owner, start, True)

    def at_home(which):
        pl.when(both(other, used(which[1])))(lambda: copy(which, here, None).wait_recv())

    def pieces_up(kind, body):
        def group_body(name, q):
            for r in range(CUT):
                body(piece(name, kind, q, r))

        groups(kind, group_body)

    def pieces_down(kind, body):
        for r in range(CUT):
            body(piece("down", kind, 0, r))

    def cast_rows(source, columns, store):
        step = min(held, 64)

        def body(i, carry):
            taken = pl.ds(pl.multiple_of(i * step, step), step)
            target = pl.ds(pl.multiple_of(here * held + i * step, step), step)
            store(target, source[taken, columns].astype(jnp.bfloat16))
            return carry

        lax.fori_loop(0, held // step, body, 0)

    def cast_up(kind):
        for m, source in enumerate((value_weight, gate_weight)):
            for q in range(many[kind]):
                first = base[kind] + q * WIDE

                def store(target, values):
                    wide[kind][q, m, target, :] = values

                cast_rows(source, slice(first, first + WIDE), store)
            if left_over[kind]:
                first = base[kind] + many[kind] * WIDE

                def store(target, values):
                    rest[kind][m, target, :] = values

                cast_rows(source, slice(first, first + left_over[kind]), store)

    def cast_down(kind):
        def store(target, values):
            down[kind][target, :] = values

        cast_rows(down_weight, slice(base[kind], base[kind] + span[kind]), store)

    def normalize(source, target):
        step = min(rows, 64)

        def body(i, carry):
            taken = pl.ds(pl.multiple_of(i * step, step), step)
            floated = source[taken, :].astype(jnp.float32)
            mean = jnp.mean(floated * floated, axis=-1, keepdims=True)
            target[taken, :] = (floated * lax.rsqrt(mean + 1e-06) * gains[0:1, :]).astype(
                jnp.bfloat16
            )
            return carry

        lax.fori_loop(0, rows // step, body, 0)

    def swap():
        return pltpu.make_async_remote_copy(
            src_ref=tokens,
            dst_ref=raw,
            send_sem=token_sem.at[0],
            recv_sem=token_sem.at[1],
            device_id={"grp": lax.rem(group + 1, parts)},
            device_id_type=MESH,
        )

    def vectors():
        return pltpu.make_async_remote_copy(
            src_ref=along,
            dst_ref=along,
            send_sem=along_sem.at[0],
            recv_sem=along_sem.at[1],
            device_id={"tp": sibling},
            device_id_type=MESH,
        )

    share = rows // pairs

    def portion(ref):
        return ref.at[pl.ds(pl.multiple_of(pair * share, share), share), :]

    def guest_copy(source, slot, target):
        return pltpu.make_async_remote_copy(
            src_ref=portion(source),
            dst_ref=portion(guest),
            send_sem=guest_send.at[slot],
            recv_sem=guest_recv.at[pair],
            device_id=target,
            device_id_type=MESH,
        )

    def lend():
        return guest_copy(tokens, pairs, {"fs": mate})

    def pass_on(k):
        return guest_copy(guest, k, {"tp": lax.rem(me + k * parts, peers)})

    def pass_across():
        return guest_copy(guest, 0, {"grp": lax.rem(group + 1, parts)})

    def relay():
        lend().wait_recv()
        pl.when(boss)(lambda: pass_across().start())
        for k in range(1, pairs):
            pass_on(k).start()

    def welcome():
        for k in range(1, pairs):
            from_pair = lax.rem(pair + k, pairs)
            landed_share = guest.at[pl.ds(pl.multiple_of(from_pair * share, share), share), :]
            pltpu.make_async_copy(landed_share, landed_share, guest_recv.at[from_pair]).wait()
        normalize(guest, guest_normed)

    def causal(weight, tap, bias, source, outer):
        up = jnp.dot(source[...], weight[...], preferred_element_type=jnp.float32)
        position = lax.broadcasted_iota(jnp.int32, up.shape, 0)
        one = jnp.where(position >= 1, pltpu.roll(up, 1, axis=0), 0.0)
        two = jnp.where(position >= 2, pltpu.roll(up, 2, axis=0), 0.0)
        return (
            along[tap : tap + 1, outer] * two
            + along[tap + 1 : tap + 2, outer] * one
            + along[tap + 2 : tap + 3, outer] * up
            + along[bias : bias + 1, outer]
        )

    def up(kind, name, q, source, keep):
        weights = wide[kind].at[q] if name == "wide" else rest[kind]
        extent = WIDE if name == "wide" else left_over[kind]
        first = q * WIDE if name == "wide" else many[kind] * WIDE
        if name == "wide":
            first = pl.multiple_of(first, WIDE)
            outer = pl.ds(pl.multiple_of(base[kind] + first, 128), extent)
        else:
            outer = pl.ds(base[kind] + first, extent)
        value = causal(weights.at[0], 0, 6, source, outer)
        gate = causal(weights.at[1], 3, 7, source, outer)
        keep[:, pl.ds(first, extent)] = (gate / (1.0 + jnp.exp(-gate)) * value).astype(jnp.bfloat16)

    def through(kind, activations, owner):
        shard = down[kind][pl.ds(pl.multiple_of(owner * held, held), held), :]
        return lax.dot_general(
            activations[...], shard, (((1,), (1,)), ((), ())), preferred_element_type=jnp.float32
        )

    def hand(source, target, owner, k, sent, received):
        peer = lax.rem(me + k, peers)
        return pltpu.make_async_remote_copy(
            src_ref=source.at[owner, pl.ds(pl.multiple_of(peer * kept, kept), kept), :],
            dst_ref=target.at[owner, block],
            send_sem=sent,
            recv_sem=received.at[owner],
            device_id={"grp": core, "tp": peer},
            device_id_type=MESH,
        )

    def hand_out(source, target, owner, sent, received):
        pl.when(other)(lambda: hand(source, target, owner, 0, sent, received).start())
        for k in range(1, peers):
            hand(source, target, owner, k, sent, received).start()

        @pl.when(boss)
        def _():
            mine = pl.ds(pl.multiple_of(me * kept, kept), kept)
            target[owner, block] = source[owner, mine, :]

    def gathered(target, owner, received):
        def some(amount):
            part = target.at[owner, pl.ds(0, amount)]
            pltpu.make_async_copy(part, part, received.at[owner]).wait()

        pl.when(boss)(lambda: some(peers - 1))
        pl.when(other)(lambda: some(peers))
        total = target[owner, 0].astype(jnp.float32)
        for k in range(1, peers):
            total = total + target[owner, k].astype(jnp.float32)
        return total

    def handed(target, sent):
        def some(amount):
            part = target.at[:, pl.ds(0, amount)]
            pltpu.make_async_copy(part, part, sent).wait()

        pl.when(boss)(lambda: some(peers - 1))
        pl.when(other)(lambda: some(peers))

    def project(owner):
        if lent:

            @pl.when(inner)
            def _():
                partial[owner] = (through(0, hidden[0], owner) + through(1, hidden[1], owner)).astype(
                    jnp.bfloat16
                )

            @pl.when(end)
            def _():
                partial[owner] = through(0, hidden[0], owner).astype(jnp.bfloat16)

        else:
            partial[owner] = through(0, hidden[0], owner).astype(jnp.bfloat16)
        hand_out(partial, landed, owner, sum_send, sum_recv)

    def guest_project(owner):
        @pl.when(helper)
        def _():
            guest_partial[owner] = through(1, guest_hidden, owner).astype(jnp.bfloat16)
            hand_out(guest_partial, guest_landed, owner, guest_sum_send, guest_sum_recv)

    def back(owner):
        return pltpu.make_async_remote_copy(
            src_ref=summed.at[owner],
            dst_ref=returned.at[owner],
            send_sem=back_send.at[owner],
            recv_sem=back_recv.at[owner],
            device_id={"fs": mate},
            device_id_type=MESH,
        )

    def give_back(owner):
        @pl.when(helper)
        def _():
            summed[owner] = gathered(guest_landed, owner, guest_sum_recv).astype(jnp.bfloat16)
            back(owner).start()

    for i, vector in enumerate((norm_gain, down_scale)):
        gains[i : i + 1, :] = vector[...].reshape(1, width)

    @pl.when(boss)
    def _():
        for i, (taps, scale, bias) in enumerate(
            ((value_taps, value_scale, value_bias), (gate_taps, gate_scale, gate_bias))
        ):
            along[3 * i : 3 * i + 3, :] = taps[...] * scale[...].reshape(1, units)
            along[6 + i : 7 + i, :] = bias[...].reshape(1, units)
        cast_up(kinds - 1)

    sides = (here == 0).astype(jnp.int32) + (here == line - 1).astype(jnp.int32)
    pl.semaphore_wait(barrier, parts * peers - 1 + 2 - sides)
    if lent:
        pl.when(both(boss, end))(lambda: lend().start())
    pl.when(boss)(lambda: swap().start())
    pieces_up(kinds - 1, lambda which: own_line(which, start))

    @pl.when(boss)
    def _():
        vectors().start()

    pieces_up(kinds - 1, lambda which: own_across(which, start))
    if lent:
        pl.when(boss)(lambda: cast_up(0))
        pieces_up(0, lambda which: own_line(which, start, True))
        pieces_up(0, lambda which: own_across(which, start))

    @pl.when(boss)
    def _():
        for kind in range(kinds):
            cast_down(kind)

    for kind in reversed(range(kinds)):
        pieces_down(kind, lambda which: own_line(which, start, True))
        pieces_down(kind, lambda which: own_across(which, start))

    if lent:
        pl.when(both(boss, helper))(relay)
    pl.when(boss)(lambda: normalize(tokens, normed))

    if lent:
        for i in range(1, line):
            pieces_up(1, lambda which: arrive(which, owner_at(i)))
            if i == 1:
                pieces_up(0, lambda which: own_line(which, start, False))

    @pl.when(other)
    def _():
        vectors().wait_recv()
        swap().wait_recv()
        normalize(raw, normed)

    if lent:
        pieces_up(1, at_home)

        @pl.when(inner)
        def _():
            groups(1, lambda name, q: up(1, name, q, normed, hidden[1]))

        pl.when(both(other, helper))(relay)

    def nearer(name, q):
        for r in range(CUT):
            at_home(piece(name, 0, q, r))
        for i in range(1, line - 1):
            for r in range(CUT):
                arrive(piece(name, 0, q, r), owner_at(i))

    groups(0, nearer)
    for kind in reversed(range(kinds)):
        pieces_down(kind, lambda which: own_line(which, start, False))

    if lent:

        @pl.when(helper)
        def _():
            welcome()
            groups(1, lambda name, q: up(1, name, q, guest_normed, guest_hidden))

    last = owner_at(line - 1)

    def farthest(name, q):
        for r in range(CUT):
            arrive(piece(name, 0, q, r), last)
        up(0, name, q, normed, hidden[0])

    groups(0, farthest)

    def finish_line(i, carry):
        owner = owner_at(i)
        for kind in reversed(range(kinds)):

            @pl.when(i == 0)
            def _():
                pieces_down(kind, at_home)

            @pl.when(i > 0)
            def _():
                pieces_down(kind, lambda which: arrive(which, owner))

            if kind:
                guest_project(owner)
        project(owner)
        if lent:
            pl.when(i > 0)(lambda: give_back(owner_at(i - 1)))
        return carry

    lax.fori_loop(0, line, finish_line, 0)
    if lent:
        give_back(last)

    def sum_up(i, carry):
        owner = owner_at(i)
        columns = pl.ds(pl.multiple_of(owner * held, held), held)
        total = gathered(landed, owner, sum_recv)

        def keep(amount):
            out[:, columns] = (amount * gains[1:2, columns]).astype(jnp.bfloat16)

        if lent:

            @pl.when(end)
            def _():
                back(owner).wait_recv()
                keep(total + returned[owner].astype(jnp.float32))

            pl.when(inner)(lambda: keep(total))
        else:
            keep(total)
        return carry

    lax.fori_loop(0, line, sum_up, 0)

    handed(landed, sum_send)

    @pl.when(boss)
    def _():
        swap().wait_send()
        vectors().wait_send()

    if lent:
        pl.when(both(boss, end))(lambda: lend().wait_send())

        @pl.when(helper)
        def _():
            pl.when(boss)(lambda: pass_across().wait_send())
            for k in range(1, pairs):
                pass_on(k).wait_send()
            handed(guest_landed, guest_sum_send)
            for owner in range(line):
                back(owner).wait_send()

    for kind in range(kinds):
        for visit in (pieces_up, pieces_down):
            visit(kind, lambda which: own_line(which, left))
            visit(kind, lambda which: own_across(which, left))
            for i in range(1, line):
                visit(kind, lambda which: onward(which, owner_at(i), left, False))


def solution(mesh):
    parts, line, peers = mesh.shape["grp"], mesh.shape["fs"], mesh.shape["tp"]

    def local(*arrays):
        rows, width = arrays[0].shape
        held, units = arrays[2].shape
        kept = rows // peers
        pairs = peers // parts
        lent = units * 5 // 11 // 128 * 128 if line >= 4 and peers > 1 else 0
        half, full = jnp.bfloat16, jnp.float32
        spans = (units - lent, lent) if lent else (units,)
        dma = pltpu.SemaphoreType.DMA
        scratch = [
            pltpu.VMEM((span // WIDE, 2, width, WIDE), half) for span in spans if span // WIDE
        ]
        scratch += [pltpu.VMEM((2, width, span % WIDE), half) for span in spans if span % WIDE]
        scratch += [pltpu.VMEM((width, span), half) for span in spans]
        scratch += [pltpu.VMEM((rows, span), half) for span in spans]
        pieces = sum((pl.cdiv(span, WIDE) + 1) * CUT for span in spans)
        scratch += [
            pltpu.VMEM((rows, width), half),
            pltpu.VMEM((rows, width), half),
            pltpu.VMEM((8, units), full),
            pltpu.VMEM((2, width), full),
            pltpu.VMEM((line, rows, held), half),
            pltpu.VMEM((line, peers, kept, held), half),
            dma((pieces, line, 3)),
            dma((pieces, line)),
            dma((2,)),
            dma((2,)),
            dma,
            dma((line,)),
        ]
        if lent:
            scratch += [
                pltpu.VMEM((rows, width), half),
                pltpu.VMEM((rows, width), half),
                pltpu.VMEM((rows, lent), half),
                pltpu.VMEM((line, rows, held), half),
                pltpu.VMEM((line, peers, kept, held), half),
                pltpu.VMEM((line, kept, held), half),
                pltpu.VMEM((line, kept, held), half),
                dma((pairs + 1,)),
                dma((pairs,)),
                dma,
                dma((line,)),
                dma((line,)),
                dma((line,)),
            ]
        return pl.pallas_call(
            functools.partial(kernel, parts, line, peers, lent),
            out_shape=jax.ShapeDtypeStruct((kept, width), half),
            in_specs=[pl.BlockSpec(memory_space=pltpu.VMEM)] * 12,
            out_specs=pl.BlockSpec(memory_space=pltpu.VMEM),
            scratch_shapes=scratch,
            compiler_params=pltpu.CompilerParams(
                collective_id=0, has_side_effects=True, vmem_limit_bytes=62 * 1024 * 1024
            ),
        )(*arrays)

    return jax.shard_map(
        local,
        mesh=mesh,
        in_specs=(
            P(("grp", "fs"), None),
            P(),
            P("fs", "tp"),
            P("fs", "tp"),
            P("fs", "tp"),
            P("tp"),
            P("tp"),
            P(),
            P(None, "tp"),
            P(None, "tp"),
            P("tp"),
            P("tp"),
        ),
        out_specs=P(("grp", "fs", "tp"), None),
        check_vma=False,
    )
```

time: 162 us -> 131 us (0.81)
  Pallas kernels: 160 us -> 128 us
    pallas_call x1, Pallas kernels: 160 us -> 128 us  [local(): pl.pallas_call(functools.partial(kernel, parts, line, peers, lent), out_s...]
where the time goes in v1:
time: 131 us; the launch traced here: 130 us
  Pallas kernels  128 us (98%)
  local copies, waits for them, and re-layouts  1.88 us (1%)
    pallas_call x1, Pallas kernels, local(): pl.pallas_call(functools.partial(kernel, parts, line, peers, lent), out_s...  128 us

profile of v1, /device:TPU:0, one launch (start us, length us, event | category | flops | bytes accessed | tf_op | source)
XLA Modules:
  0.0 129.7 jit_solution(5871086526578975101)
XLA Ops:
  0.0 127.8 %shard_map.118 = bf16[128,2048]{1,0:T(8,128)(2,1)} custom-call(bf16[512,2048]{1,0:T(8,128)(2,1)} %tokens.1, f32[2048]{0:T(1024)} %norm_gain.1, f32[512,1408]{1,0:T(8,128)} %value_weight.1, f32[512,1408]{1,0:T(8,128)} %gate_weight.1, f32[512,1408]{1,0:T(8,128)} %down_weight.1, f32[1408]{0:T(1024)} %value_scale.1, f32[1408]{0:T(1024)} %gate_scale.1, ...), custom_call_target="tpu_custom_call" | custom-call | tf_op jit(solution)/shard_map/pallas_call | solution.py:621
  127.8 1.9 %copy.14 = bf16[128,2048]{1,0:T(8,128)(2,1)} copy(bf16[128,2048]{1,0:T(8,128)(2,1)} %shard_map.118) | data formatting | bytes 1048576

commit v2 on v1

--- a/solution.py
+++ b/solution.py
@@ -17,6 +17,7 @@
     line,
     peers,
     lent,
+    slices,
     tokens,
     norm_gain,
     value_weight,
@@ -38,6 +39,7 @@
     kinds = 2 if lent else 1
     rows, width = tokens.shape
     held, units = value_weight.shape
+    thin = held // slices
     kept = rows // peers
     pairs = peers // parts
     base = (0, units - lent)
@@ -48,8 +50,9 @@
     rest = [take(1)[0] if left_over[k] else None for k in range(kinds)]
     down = take(kinds)
     hidden = take(kinds)
+    value_load, gate_load, down_load, token_load = take(4)
     raw, normed, along, gains, partial, landed = take(6)
-    send_sem, recv_sem, token_sem, along_sem, sum_send, sum_recv = take(6)
+    send_sem, recv_sem, load_sem, token_sem, along_sem, sum_send, sum_recv = take(7)
     if lent:
         guest, guest_normed, guest_hidden, guest_partial, guest_landed, summed, returned = take(7)
         guest_send, guest_recv, guest_sum_send, guest_sum_recv, back_send, back_recv = take(6)
@@ -84,26 +87,33 @@
         first = jnp.where(i > 2 * near, i, turned)
         return jnp.where(here < line // 2, first, line - 1 - first)
 
-    numbers = {}
+    def slice_at(j):
+        return owner_at(j // slices) * slices + j % slices
+
+    numbers, stores = {}, {}
     count = 0
     for k in range(kinds):
-        for name, amount in (("wide", many[k]), ("rest", 1 if left_over[k] else 0), ("down", 1)):
+        for name, amount in (("wide", many[k] * CUT), ("rest", CUT), ("down", slices)):
+            stores[name, k] = len(stores)
             numbers[name, k] = count
-            count += amount * CUT
+            count += amount if name != "rest" or left_over[k] else 0
+
+    def store_rows(name, kind, taken):
+        if name == "wide":
+            return wide[kind].at[:, :, taken, :]
+        if name == "rest":
+            return rest[kind].at[:, taken, :]
+        return down[kind].at[taken, :]
 
     def piece(name, kind, q, r):
-        number = numbers[name, kind] + q * CUT + r
+        cut = slices if name == "down" else CUT
 
         def ref(owner):
-            part = held // CUT
-            first = pl.multiple_of(owner * held + r * part, part)
-            if name == "wide":
-                return wide[kind].at[q, :, pl.ds(first, part), :]
-            if name == "rest":
-                return rest[kind].at[:, pl.ds(first, part), :]
-            return down[kind].at[pl.ds(first, part), :]
-
-        return number, kind, ref
+            part = held // cut
+            taken = pl.ds(pl.multiple_of(owner * held + r * part, part), part)
+            return wide[kind].at[q, :, taken, :] if name == "wide" else store_rows(name, kind, taken)
+
+        return numbers[name, kind] + q * CUT + r, kind, ref, stores[name, kind]
 
     def groups(kind, body):
         if many[kind]:
@@ -117,7 +127,7 @@
             body("rest", 0)
 
     def copy(which, owner, direction):
-        number, kind, ref = which
+        number, kind, ref, store = which
         if direction is None:
             target, lane = {"tp": sibling}, 2
         else:
@@ -126,7 +136,7 @@
         return pltpu.make_async_remote_copy(
             src_ref=ref(owner),
             dst_ref=ref(owner),
-            send_sem=send_sem.at[number, owner, lane],
+            send_sem=send_sem.at[store, lane],
             recv_sem=recv_sem.at[number, owner],
             device_id=target,
             device_id_type=MESH,
@@ -139,43 +149,33 @@
         there = here + direction
         return both(there >= kind, there <= line - 1 - kind)
 
-    def start(dma):
-        dma.start()
-
-    def left(dma):
-        dma.wait_send()
-
     def toward_end(direction):
         there = here + direction
         return jnp.logical_or(end, jnp.logical_or(there == 0, there == line - 1))
 
-    def own_line(which, act, early=None):
+    def own_line(which, early=None):
         for direction in (1, -1):
             go = both(boss, further(which[1], direction))
             if early is True:
                 go = both(go, toward_end(direction))
             elif early is False:
                 go = both(go, jnp.logical_not(toward_end(direction)))
-            pl.when(go)(lambda: act(copy(which, here, direction)))
-
-    def own_across(which, act):
-        pl.when(both(boss, used(which[1])))(lambda: act(copy(which, here, None)))
-
-    def onward(which, owner, act, arrive):
+            pl.when(go)(lambda: copy(which, here, direction).start())
+
+    def own_across(which):
+        pl.when(both(boss, used(which[1])))(lambda: copy(which, here, None).start())
+
+    def arrive(which, owner):
         direction = jnp.where(owner < here, 1, -1)
 
         @pl.when(used(which[1]))
         def _():
-            if arrive:
-                copy(which, owner, None).wait_recv()
+            copy(which, owner, None).wait_recv()
 
             @pl.when(boss)
             def _():
-                pl.when(further(which[1], direction))(lambda: act(copy(which, owner, direction)))
-                act(copy(which, owner, None))
-
-    def arrive(which, owner):
-        onward(which, owner, start, True)
+                pl.when(further(which[1], direction))(lambda: copy(which, owner, direction).start())
+                copy(which, owner, None).start()
 
     def at_home(which):
         pl.when(both(other, used(which[1])))(lambda: copy(which, here, None).wait_recv())
@@ -188,7 +188,7 @@
         groups(kind, group_body)
 
     def pieces_down(kind, body):
-        for r in range(CUT):
+        for r in range(slices):
             body(piece("down", kind, 0, r))
 
     def cast_rows(source, columns, store):
@@ -202,28 +202,40 @@
 
         lax.fori_loop(0, held // step, body, 0)
 
-    def cast_up(kind):
-        for m, source in enumerate((value_weight, gate_weight)):
-            for q in range(many[kind]):
+    def load(number):
+        if number < 2 * kinds:
+            kind = kinds - 1 - number // 2
+            columns = pl.ds(base[kind], span[kind])
+            source, target = ((value_weight, value_load), (gate_weight, gate_load))[number % 2]
+            source, target = source.at[:, columns], target.at[:, columns]
+        elif number == 2 * kinds:
+            source, target = tokens, token_load
+        else:
+            source, target = down_weight, down_load
+        return pltpu.make_async_copy(source, target, load_sem.at[number])
+
+    def loaded(kind):
+        for m in range(2):
+            load(2 * (kinds - 1 - kind) + m).wait()
+
+    def cast_up(kind, begin, stop):
+        for m, source in enumerate((value_load, gate_load)):
+            for q in range(begin, stop):
                 first = base[kind] + q * WIDE
 
                 def store(target, values):
-                    wide[kind][q, m, target, :] = values
-
-                cast_rows(source, slice(first, first + WIDE), store)
-            if left_over[kind]:
-                first = base[kind] + many[kind] * WIDE
-
-                def store(target, values):
-                    rest[kind][m, target, :] = values
-
-                cast_rows(source, slice(first, first + left_over[kind]), store)
+                    if q < many[kind]:
+                        wide[kind][q, m, target, :] = values
+                    else:
+                        rest[kind][m, target, :] = values
+
+                cast_rows(source, slice(first, min(first + WIDE, base[kind] + span[kind])), store)
 
     def cast_down(kind):
         def store(target, values):
             down[kind][target, :] = values
 
-        cast_rows(down_weight, slice(base[kind], base[kind] + span[kind]), store)
+        cast_rows(down_load, slice(base[kind], base[kind] + span[kind]), store)
 
     def normalize(source, target):
         step = min(rows, 64)
@@ -239,12 +251,13 @@
 
         lax.fori_loop(0, rows // step, body, 0)
 
-    def swap():
+    def swap(part):
+        taken = pl.ds(part * (rows // 2), rows // 2)
         return pltpu.make_async_remote_copy(
-            src_ref=tokens,
-            dst_ref=raw,
-            send_sem=token_sem.at[0],
-            recv_sem=token_sem.at[1],
+            src_ref=token_load.at[taken, :],
+            dst_ref=raw.at[taken, :],
+            send_sem=token_sem.at[part],
+            recv_sem=token_sem.at[2 + part],
             device_id={"grp": lax.rem(group + 1, parts)},
             device_id_type=MESH,
         )
@@ -275,7 +288,7 @@
         )
 
     def lend():
-        return guest_copy(tokens, pairs, {"fs": mate})
+        return guest_copy(token_load, pairs, {"fs": mate})
 
     def pass_on(k):
         return guest_copy(guest, k, {"tp": lax.rem(me + k * parts, peers)})
@@ -286,6 +299,7 @@
     def relay():
         lend().wait_recv()
         pl.when(boss)(lambda: pass_across().start())
+        pl.when(boss)(lambda: swap(1).start())
         for k in range(1, pairs):
             pass_on(k).start()
 
@@ -322,7 +336,7 @@
         keep[:, pl.ds(first, extent)] = (gate / (1.0 + jnp.exp(-gate)) * value).astype(jnp.bfloat16)
 
     def through(kind, activations, owner):
-        shard = down[kind][pl.ds(pl.multiple_of(owner * held, held), held), :]
+        shard = down[kind][pl.ds(pl.multiple_of(owner * thin, thin), thin), :]
         return lax.dot_general(
             activations[...], shard, (((1,), (1,)), ((), ())), preferred_element_type=jnp.float32
         )
@@ -395,7 +409,7 @@
         return pltpu.make_async_remote_copy(
             src_ref=summed.at[owner],
             dst_ref=returned.at[owner],
-            send_sem=back_send.at[owner],
+            send_sem=back_send,
             recv_sem=back_recv.at[owner],
             device_id={"fs": mate},
             device_id_type=MESH,
@@ -407,123 +421,184 @@
             summed[owner] = gathered(guest_landed, owner, guest_sum_recv).astype(jnp.bfloat16)
             back(owner).start()
 
-    for i, vector in enumerate((norm_gain, down_scale)):
-        gains[i : i + 1, :] = vector[...].reshape(1, width)
+    scope = jax.named_scope
 
     @pl.when(boss)
     def _():
-        for i, (taps, scale, bias) in enumerate(
-            ((value_taps, value_scale, value_bias), (gate_taps, gate_scale, gate_bias))
-        ):
-            along[3 * i : 3 * i + 3, :] = taps[...] * scale[...].reshape(1, units)
-            along[6 + i : 7 + i, :] = bias[...].reshape(1, units)
-        cast_up(kinds - 1)
-
-    sides = (here == 0).astype(jnp.int32) + (here == line - 1).astype(jnp.int32)
-    pl.semaphore_wait(barrier, parts * peers - 1 + 2 - sides)
+        for number in (*range(2), 2 * kinds, 2 * kinds + 1, *range(2, 2 * kinds)):
+            load(number).start()
+
+    with scope("vectors"):
+        for i, vector in enumerate((norm_gain, down_scale)):
+            gains[i : i + 1, :] = vector[...].reshape(1, width)
+
+        @pl.when(boss)
+        def _():
+            for i, (taps, scale, bias) in enumerate(
+                ((value_taps, value_scale, value_bias), (gate_taps, gate_scale, gate_bias))
+            ):
+                along[3 * i : 3 * i + 3, :] = taps[...] * scale[...].reshape(1, units)
+                along[6 + i : 7 + i, :] = bias[...].reshape(1, units)
+
+    amounts = [many[k] + (1 if left_over[k] else 0) for k in range(kinds)]
+    first = ("wide", 0) if many[0] else ("rest", 0)
+
+    def others(body):
+        if many[0] > 1:
+
+            def one(q, carry):
+                body("wide", q)
+                return carry
+
+            lax.fori_loop(1, many[0], one, 0)
+        if left_over[0] and many[0]:
+            body("rest", 0)
+
+    def each(name, q, body):
+        for r in range(CUT):
+            body(piece(name, 0, q, r))
+
+    with scope("cast_first"):
+
+        @pl.when(boss)
+        def _():
+            loaded(kinds - 1)
+            cast_up(kinds - 1, 0, amounts[-1])
+
+    with scope("barrier"):
+        sides = (here == 0).astype(jnp.int32) + (here == line - 1).astype(jnp.int32)
+        pl.semaphore_wait(barrier, parts * peers - 1 + 2 - sides)
+    with scope("send_first"):
+        if lent:
+
+            @pl.when(both(boss, end))
+            def _():
+                load(2 * kinds).wait()
+                lend().start()
+
+        pieces_up(kinds - 1, own_line)
+
+        @pl.when(boss)
+        def _():
+            pl.when(inner if lent else boss)(lambda: load(2 * kinds).wait())
+            swap(0).start()
+            pl.when(jnp.logical_not(helper) if lent else boss)(lambda: swap(1).start())
+            vectors().start()
+
+        pieces_up(kinds - 1, own_across)
+    with scope("cast_rest"):
+        if lent:
+
+            @pl.when(boss)
+            def _():
+                loaded(0)
+                cast_up(0, 0, 1)
+
+            each(*first, own_line)
+        pl.when(boss)(lambda: load(2 * kinds + 1).wait())
+        if lent:
+            pl.when(boss)(lambda: cast_down(1))
+            pieces_down(1, lambda which: own_line(which, True))
+            pl.when(boss)(lambda: cast_up(0, 1, amounts[0]))
+            others(lambda name, q: each(name, q, lambda which: own_line(which, True)))
+            pieces_up(0, own_across)
+        pl.when(boss)(lambda: cast_down(0))
+        pieces_down(0, lambda which: own_line(which, True))
+        for kind in reversed(range(kinds)):
+            pieces_down(kind, own_across)
+
+    with scope("normalize"):
+        pl.when(boss)(lambda: normalize(token_load, normed))
+
+    last = owner_at(line - 1)
+
+    def nearer(name, q):
+        with scope("a_near"):
+            each(name, q, at_home)
+            for i in reversed(range(1, line - 1)):
+                each(name, q, lambda which: arrive(which, owner_at(i)))
+
+    def farthest(name, q):
+        with scope("a_far"):
+            each(name, q, lambda which: arrive(which, last))
+
     if lent:
-        pl.when(both(boss, end))(lambda: lend().start())
-    pl.when(boss)(lambda: swap().start())
-    pieces_up(kinds - 1, lambda which: own_line(which, start))
-
-    @pl.when(boss)
-    def _():
-        vectors().start()
-
-    pieces_up(kinds - 1, lambda which: own_across(which, start))
+        with scope("relay"):
+            pl.when(helper)(relay)
+
+        def b_near(which):
+            for i in range(1, line - 1):
+                arrive(which, owner_at(i))
+
+        with scope("b_near"):
+            pieces_up(1, b_near)
+
+    nearer(*first)
     if lent:
-        pl.when(boss)(lambda: cast_up(0))
-        pieces_up(0, lambda which: own_line(which, start, True))
-        pieces_up(0, lambda which: own_across(which, start))
-
-    @pl.when(boss)
-    def _():
-        for kind in range(kinds):
-            cast_down(kind)
-
-    for kind in reversed(range(kinds)):
-        pieces_down(kind, lambda which: own_line(which, start, True))
-        pieces_down(kind, lambda which: own_across(which, start))
+        others(lambda name, q: each(name, q, lambda which: own_line(which, False)))
+
+    with scope("other_tokens"):
+
+        @pl.when(other)
+        def _():
+            vectors().wait_recv()
+            swap(0).wait_recv()
+            swap(1).wait_recv()
+            normalize(raw, normed)
 
     if lent:
-        pl.when(both(boss, helper))(relay)
-    pl.when(boss)(lambda: normalize(tokens, normed))
-
+        with scope("b_far"):
+            pieces_up(1, at_home)
+            pieces_up(1, lambda which: arrive(which, last))
+        with scope("b_own"):
+
+            @pl.when(inner)
+            def _():
+                groups(1, lambda name, q: up(1, name, q, normed, hidden[1]))
+    farthest(*first)
     if lent:
-        for i in range(1, line):
-            pieces_up(1, lambda which: arrive(which, owner_at(i)))
-            if i == 1:
-                pieces_up(0, lambda which: own_line(which, start, False))
-
-    @pl.when(other)
-    def _():
-        vectors().wait_recv()
-        swap().wait_recv()
-        normalize(raw, normed)
-
+        with scope("guest_wait"):
+            pl.when(helper)(welcome)
+        with scope("b_guest"):
+
+            @pl.when(helper)
+            def _():
+                groups(1, lambda name, q: up(1, name, q, guest_normed, guest_hidden))
+
+    def guest_early():
+        with scope("guest_early"):
+            pieces_down(1, at_home)
+            pieces_down(1, lambda which: arrive(which, owner_at(1)))
+
+            def early(j, carry):
+                guest_project(slice_at(j))
+                return carry
+
+            lax.fori_loop(0, 2 * slices, early, 0)
+
+    others(nearer)
     if lent:
-        pieces_up(1, at_home)
-
-        @pl.when(inner)
-        def _():
-            groups(1, lambda name, q: up(1, name, q, normed, hidden[1]))
-
-        pl.when(both(other, helper))(relay)
-
-    def nearer(name, q):
-        for r in range(CUT):
-            at_home(piece(name, 0, q, r))
-        for i in range(1, line - 1):
-            for r in range(CUT):
-                arrive(piece(name, 0, q, r), owner_at(i))
-
-    groups(0, nearer)
-    for kind in reversed(range(kinds)):
-        pieces_down(kind, lambda which: own_line(which, start, False))
-
-    if lent:
-
-        @pl.when(helper)
-        def _():
-            welcome()
-            groups(1, lambda name, q: up(1, name, q, guest_normed, guest_hidden))
-
-    last = owner_at(line - 1)
-
-    def farthest(name, q):
-        for r in range(CUT):
-            arrive(piece(name, 0, q, r), last)
-        up(0, name, q, normed, hidden[0])
-
-    groups(0, farthest)
-
-    def finish_line(i, carry):
-        owner = owner_at(i)
-        for kind in reversed(range(kinds)):
-
-            @pl.when(i == 0)
-            def _():
-                pieces_down(kind, at_home)
-
-            @pl.when(i > 0)
-            def _():
-                pieces_down(kind, lambda which: arrive(which, owner))
-
-            if kind:
-                guest_project(owner)
-        project(owner)
-        if lent:
-            pl.when(i > 0)(lambda: give_back(owner_at(i - 1)))
-        return carry
-
-    lax.fori_loop(0, line, finish_line, 0)
-    if lent:
-        give_back(last)
-
-    def sum_up(i, carry):
-        owner = owner_at(i)
-        columns = pl.ds(pl.multiple_of(owner * held, held), held)
-        total = gathered(landed, owner, sum_recv)
+        guest_early()
+
+    def own_down(begin, stop):
+        for r in range(begin, stop):
+            for kind in range(kinds):
+                own_line(piece("down", kind, 0, r), False)
+
+    def own_up(name, q):
+        final = q == many[0] - 1 if not left_over[0] else here < (line if name == "rest" else 0)
+        pl.when(final)(lambda: own_down(0, 1))
+        if name == "wide" or many[0]:
+            pl.when(jnp.logical_or(name == "rest", q > 0))(lambda: farthest(name, q))
+        pl.when(final)(lambda: own_down(1, slices))
+        with scope("a_own"):
+            up(0, name, q, normed, hidden[0])
+
+    groups(0, own_up)
+
+    def collect(at):
+        columns = pl.ds(pl.multiple_of(at * thin, thin), thin)
+        total = gathered(landed, at, sum_recv)
 
         def keep(amount):
             out[:, columns] = (amount * gains[1:2, columns]).astype(jnp.bfloat16)
@@ -532,41 +607,94 @@
 
             @pl.when(end)
             def _():
-                back(owner).wait_recv()
-                keep(total + returned[owner].astype(jnp.float32))
+                back(at).wait_recv()
+                keep(total + returned[at].astype(jnp.float32))
 
             pl.when(inner)(lambda: keep(total))
         else:
             keep(total)
+
+    total_slices = line * slices
+    lag = min(2 * slices, total_slices)
+    late = max(slices - 1, 1)
+
+    def finish_line(j, carry):
+        i, r = j // slices, j % slices
+        owner = owner_at(i)
+        for kind in range(kinds):
+            which = piece("down", kind, 0, r)
+            with scope(f"c_arrive#k={kind}"):
+                if kind:
+                    pl.when(i > 1)(lambda: arrive(which, owner))
+                else:
+                    pl.when(i == 0)(lambda: at_home(which))
+                    pl.when(i > 0)(lambda: arrive(which, owner))
+        if lent:
+            with scope("c_guest"):
+                pl.when(i > 1)(lambda: guest_project(owner * slices + r))
+            with scope("give_back"):
+                pl.when(i < 2)(lambda: give_back(slice_at(j)))
+        with scope("c_own"):
+            project(owner * slices + r)
+        if lent:
+            with scope("give_back"):
+                pl.when(j >= 2 * slices + late)(lambda: give_back(slice_at(j - late)))
+        with scope("collect"):
+            pl.when(j >= lag)(lambda: collect(slice_at(j - lag)))
         return carry
 
-    lax.fori_loop(0, line, sum_up, 0)
-
-    handed(landed, sum_send)
-
-    @pl.when(boss)
-    def _():
-        swap().wait_send()
-        vectors().wait_send()
+    lax.fori_loop(0, total_slices, finish_line, 0)
 
     if lent:
-        pl.when(both(boss, end))(lambda: lend().wait_send())
-
-        @pl.when(helper)
-        def _():
-            pl.when(boss)(lambda: pass_across().wait_send())
-            for k in range(1, pairs):
-                pass_on(k).wait_send()
-            handed(guest_landed, guest_sum_send)
-            for owner in range(line):
-                back(owner).wait_send()
-
-    for kind in range(kinds):
-        for visit in (pieces_up, pieces_down):
-            visit(kind, lambda which: own_line(which, left))
-            visit(kind, lambda which: own_across(which, left))
-            for i in range(1, line):
-                visit(kind, lambda which: onward(which, owner_at(i), left, False))
+
+
+        def give_rest(j, carry):
+            with scope("give_rest"):
+                give_back(slice_at(j))
+            return carry
+
+        lax.fori_loop(total_slices - late, total_slices, give_rest, 0)
+
+    def rest_of_line(j, carry):
+        with scope("collect_rest"):
+            collect(slice_at(j))
+        return carry
+
+    lax.fori_loop(total_slices - lag, total_slices, rest_of_line, 0)
+
+    def departed(name, kind, amount, lane):
+        part = store_rows(name, kind, pl.ds(0, amount * held))
+        pltpu.make_async_copy(part, part, send_sem.at[stores[name, kind], lane]).wait()
+
+    with scope("left"):
+        handed(landed, sum_send)
+
+        @pl.when(boss)
+        def _():
+            swap(0).wait_send()
+            swap(1).wait_send()
+            vectors().wait_send()
+            for kind in range(kinds):
+                for name, there in (("wide", many[kind]), ("rest", left_over[kind]), ("down", 1)):
+                    if there:
+                        for lane, direction in ((0, 1), (1, -1)):
+                            amount = here + 1 if direction > 0 else line - here
+                            for some in range(1, line):
+                                pl.when(both(amount == some, further(kind, direction)))(
+                                    lambda: departed(name, kind, some, lane)
+                                )
+                        pl.when(used(kind))(lambda: departed(name, kind, line, 2))
+
+        if lent:
+            pl.when(both(boss, end))(lambda: lend().wait_send())
+
+            @pl.when(helper)
+            def _():
+                pl.when(boss)(lambda: pass_across().wait_send())
+                for k in range(1, pairs):
+                    pass_on(k).wait_send()
+                handed(guest_landed, guest_sum_send)
+                pltpu.make_async_copy(summed, summed, back_send).wait()
 
 
 def solution(mesh):
@@ -577,7 +705,9 @@
         held, units = arrays[2].shape
         kept = rows // peers
         pairs = peers // parts
-        lent = units * 5 // 11 // 128 * 128 if line >= 4 and peers > 1 else 0
+        lent = units * 6 // 11 // 128 * 128 if line >= 4 and peers > 1 else 0
+        slices = 4 if held % 512 == 0 else 1
+        thin = held // slices
         half, full = jnp.bfloat16, jnp.float32
         spans = (units - lent, lent) if lent else (units,)
         dma = pltpu.SemaphoreType.DMA
@@ -587,41 +717,49 @@
         scratch += [pltpu.VMEM((2, width, span % WIDE), half) for span in spans if span % WIDE]
         scratch += [pltpu.VMEM((width, span), half) for span in spans]
         scratch += [pltpu.VMEM((rows, span), half) for span in spans]
-        pieces = sum((pl.cdiv(span, WIDE) + 1) * CUT for span in spans)
+        pieces = sum(pl.cdiv(span, WIDE) * CUT + slices for span in spans)
         scratch += [
+            pltpu.VMEM((held, units), full),
+            pltpu.VMEM((held, units), full),
+            pltpu.VMEM((held, units), full),
+            pltpu.VMEM((rows, width), half),
             pltpu.VMEM((rows, width), half),
             pltpu.VMEM((rows, width), half),
             pltpu.VMEM((8, units), full),
             pltpu.VMEM((2, width), full),
-            pltpu.VMEM((line, rows, held), half),
-            pltpu.VMEM((line, peers, kept, held), half),
-            dma((pieces, line, 3)),
+            pltpu.VMEM((line * slices, rows, thin), half),
+            pltpu.VMEM((line * slices, peers, kept, thin), half),
+            dma((3 * len(spans), 3)),
             dma((pieces, line)),
-            dma((2,)),
+            dma((2 * len(spans) + 2,)),
+            dma((4,)),
             dma((2,)),
             dma,
-            dma((line,)),
+            dma((line * slices,)),
         ]
         if lent:
             scratch += [
                 pltpu.VMEM((rows, width), half),
                 pltpu.VMEM((rows, width), half),
                 pltpu.VMEM((rows, lent), half),
-                pltpu.VMEM((line, rows, held), half),
-                pltpu.VMEM((line, peers, kept, held), half),
-                pltpu.VMEM((line, kept, held), half),
-                pltpu.VMEM((line, kept, held), half),
+                pltpu.VMEM((line * slices, rows, thin), half),
+                pltpu.VMEM((line * slices, peers, kept, thin), half),
+                pltpu.VMEM((line * slices, kept, thin), half),
+                pltpu.VMEM((line * slices, kept, thin), half),
                 dma((pairs + 1,)),
                 dma((pairs,)),
                 dma,
-                dma((line,)),
-                dma((line,)),
-                dma((line,)),
+                dma((line * slices,)),
+                dma,
+                dma((line * slices,)),
             ]
         return pl.pallas_call(
-            functools.partial(kernel, parts, line, peers, lent),
+            functools.partial(kernel, parts, line, peers, lent, slices),
             out_shape=jax.ShapeDtypeStruct((kept, width), half),
-            in_specs=[pl.BlockSpec(memory_space=pltpu.VMEM)] * 12,
+            in_specs=[
+                pl.BlockSpec(memory_space=pl.ANY if i in (0, 2, 3, 4) else pltpu.VMEM)
+                for i in range(12)
+            ],
             out_specs=pl.BlockSpec(memory_space=pltpu.VMEM),
             scratch_shapes=scratch,
             compiler_params=pltpu.CompilerParams(

time: 131 us -> 118 us (0.901); the launches traced: 130 us -> 118 us
  Pallas kernels: 128 us -> 116 us
    pallas_call x1, Pallas kernels: 128 us -> 116 us  [local(): pl.pallas_call(functools.partial(kernel, parts, line, peers, lent, slices...]
where the time goes in v2:
time: 118 us
  Pallas kernels  116 us (98%)
  local copies, waits for them, and re-layouts  1.88 us (2%)
    pallas_call x1, Pallas kernels, local(): pl.pallas_call(functools.partial(kernel, parts, line, peers, lent, slices...  116 us

profile of v2, /device:TPU:0, one launch (start us, length us, event | category | flops | bytes accessed | tf_op | source)
XLA Modules:
  0.0 118.0 jit_solution(11854519402419789934)
XLA Ops:
  0.0 116.1 %shard_map.118 = bf16[128,2048]{1,0:T(8,128)(2,1)} custom-call(bf16[512,2048]{1,0:T(8,128)(2,1)} %tokens.1, f32[2048]{0:T(1024)} %norm_gain.1, f32[512,1408]{1,0:T(8,128)} %value_weight.1, f32[512,1408]{1,0:T(8,128)} %gate_weight.1, f32[512,1408]{1,0:T(8,128)} %down_weight.1, f32[1408]{0:T(1024)} %value_scale.1, f32[1408]{0:T(1024)} %gate_scale.1, ...), custom_call_target="tpu_custom_call" | custom-call | tf_op jit(solution)/shard_map/pallas_call | solution.py:756
  116.1 1.9 %copy.14 = bf16[128,2048]{1,0:T(8,128)(2,1)} copy(bf16[128,2048]{1,0:T(8,128)(2,1)} %shard_map.118) | data formatting | bytes 1048576

commit v3 on v2

--- a/solution.py
+++ b/solution.py
@@ -51,11 +51,13 @@
     down = take(kinds)
     hidden = take(kinds)
     value_load, gate_load, down_load, token_load = take(4)
-    raw, normed, along, gains, partial, landed = take(6)
-    send_sem, recv_sem, load_sem, token_sem, along_sem, sum_send, sum_recv = take(7)
+    raw, normed, along, gains, partial, landed, x_stage = take(7)
+    send_sem, recv_sem, load_sem, token_sem, along_sem = take(5)
+    sum_send, sum_recv, x_send, x_recv = take(4)
     if lent:
-        guest, guest_normed, guest_hidden, guest_partial, guest_landed, summed, returned = take(7)
-        guest_send, guest_recv, guest_sum_send, guest_sum_recv, back_send, back_recv = take(6)
+        guest, guest_normed, guest_hidden, guest_partial, guest_landed, y_stage = take(6)
+        summed, returned, guest_send, guest_recv, back_send, back_recv = take(6)
+        guest_sum_send, guest_direct, guest_sum_recv, y_send, y_recv = take(5)
 
     pair = lax.div(me, parts)
     core = lax.rem(me, parts)
@@ -87,8 +89,13 @@
         first = jnp.where(i > 2 * near, i, turned)
         return jnp.where(here < line // 2, first, line - 1 - first)
 
+    def turn(p):
+        if line != 4:
+            return owner_at(p)
+        return owner_at(jnp.where(p < 2, p, 5 - p))
+
     def slice_at(j):
-        return owner_at(j // slices) * slices + j % slices
+        return turn(j // slices) * slices + j % slices
 
     numbers, stores = {}, {}
     count = 0
@@ -165,6 +172,17 @@
     def own_across(which):
         pl.when(both(boss, used(which[1])))(lambda: copy(which, here, None).start())
 
+    def arrive_here(which, owner):
+        @pl.when(used(which[1]))
+        def _():
+            copy(which, owner, None).wait_recv()
+            pl.when(boss)(lambda: copy(which, owner, None).start())
+
+    def pass_along(which, owner):
+        direction = jnp.where(owner < here, 1, -1)
+        go = both(both(boss, used(which[1])), further(which[1], direction))
+        pl.when(go)(lambda: copy(which, owner, direction).start())
+
     def arrive(which, owner):
         direction = jnp.where(owner < here, 1, -1)
 
@@ -341,48 +359,103 @@
             activations[...], shard, (((1,), (1,)), ((), ())), preferred_element_type=jnp.float32
         )
 
-    def hand(source, target, owner, k, sent, received):
-        peer = lax.rem(me + k, peers)
+    def hand(source, target, at, slot, to_group, peer, sent, received):
         return pltpu.make_async_remote_copy(
-            src_ref=source.at[owner, pl.ds(pl.multiple_of(peer * kept, kept), kept), :],
-            dst_ref=target.at[owner, block],
+            src_ref=source.at[at, pl.ds(pl.multiple_of(peer * kept, kept), kept), :],
+            dst_ref=target.at[at, slot],
             send_sem=sent,
-            recv_sem=received.at[owner],
-            device_id={"grp": core, "tp": peer},
+            recv_sem=received.at[at],
+            device_id={"grp": to_group, "tp": peer},
             device_id_type=MESH,
         )
 
-    def hand_out(source, target, owner, sent, received):
-        pl.when(other)(lambda: hand(source, target, owner, 0, sent, received).start())
-        for k in range(1, peers):
-            hand(source, target, owner, k, sent, received).start()
+    mine = pl.ds(pl.multiple_of(me * kept, kept), kept)
+    folded = (line - 1) * slices
+
+    def direct(source, target, at, sent, received):
+        for k in range(peers):
+            peer = lax.rem(me + k, peers)
+            copy_out = hand(source, target, at, block, core, peer, sent, received)
+            pl.when(other if k == 0 else here >= 0)(lambda: copy_out.start())
 
         @pl.when(boss)
         def _():
-            mine = pl.ds(pl.multiple_of(me * kept, kept), kept)
-            target[owner, block] = source[owner, mine, :]
-
-    def gathered(target, owner, received):
+            target[at, block] = source[at, mine, :]
+
+    def across(at):
+        return pltpu.make_async_remote_copy(
+            src_ref=partial.at[at],
+            dst_ref=x_stage.at[at],
+            send_sem=x_send,
+            recv_sem=x_recv.at[at],
+            device_id={"grp": lax.rem(group + 1, parts)},
+            device_id_type=MESH,
+        )
+
+    def fold(at):
+        @pl.when(boss)
+        def _():
+            across(at).wait_recv()
+            total = partial[at].astype(jnp.float32) + x_stage[at].astype(jnp.float32)
+            partial[at] = total.astype(jnp.bfloat16)
+            for k in range(1, peers):
+                peer = lax.rem(me + k, peers)
+                hand(partial, landed, at, pair, group, peer, sum_send, sum_recv).start()
+            landed[at, pair] = partial[at, mine, :]
+
+    pair_rows = parts * kept
+
+    def beside(at, k):
+        there = pl.multiple_of(lax.rem(pair + k, pairs) * pair_rows, pair_rows)
+        return pltpu.make_async_remote_copy(
+            src_ref=guest_partial.at[at, pl.ds(there, pair_rows), :],
+            dst_ref=y_stage.at[at, k - 1],
+            send_sem=y_send,
+            recv_sem=y_recv.at[at],
+            device_id={"tp": lax.rem(me + k * parts, peers)},
+            device_id_type=MESH,
+        )
+
+    def guest_fold(at):
+        ours = pl.ds(pl.multiple_of(pair * pair_rows, pair_rows), pair_rows)
+
+        @pl.when(helper)
+        def _():
+            if pairs > 1:
+                staged = y_stage.at[at, pl.ds(0, pairs - 1)]
+                pltpu.make_async_copy(staged, staged, y_recv.at[at]).wait()
+                total = guest_partial[at, ours, :].astype(jnp.float32)
+                for k in range(1, pairs):
+                    total = total + y_stage[at, k - 1].astype(jnp.float32)
+                guest_partial[at, ours, :] = total.astype(jnp.bfloat16)
+            for k in range(parts):
+                peer = pair * parts + lax.rem(core + k, parts)
+                copy_out = hand(
+                    guest_partial, guest_landed, at, group, core, peer, guest_sum_send, guest_sum_recv
+                )
+                pl.when(other if k == 0 else here >= 0)(lambda: copy_out.start())
+
+            @pl.when(boss)
+            def _():
+                guest_landed[at, group] = guest_partial[at, mine, :]
+
+    def gathered(target, at, slots, received):
         def some(amount):
-            part = target.at[owner, pl.ds(0, amount)]
-            pltpu.make_async_copy(part, part, received.at[owner]).wait()
-
-        pl.when(boss)(lambda: some(peers - 1))
-        pl.when(other)(lambda: some(peers))
-        total = target[owner, 0].astype(jnp.float32)
-        for k in range(1, peers):
-            total = total + target[owner, k].astype(jnp.float32)
+            if amount:
+                part = target.at[at, pl.ds(0, amount)]
+                pltpu.make_async_copy(part, part, received.at[at]).wait()
+
+        pl.when(boss)(lambda: some(slots - 1))
+        pl.when(other)(lambda: some(slots))
+        total = target[at, 0].astype(jnp.float32)
+        for k in range(1, slots):
+            total = total + target[at, k].astype(jnp.float32)
         return total
 
-    def handed(target, sent):
-        def some(amount):
-            part = target.at[:, pl.ds(0, amount)]
-            pltpu.make_async_copy(part, part, sent).wait()
-
-        pl.when(boss)(lambda: some(peers - 1))
-        pl.when(other)(lambda: some(peers))
-
-    def project(owner):
+    def handed(part, sent):
+        pltpu.make_async_copy(part, part, sent).wait()
+
+    def project(owner, is_last):
         if lent:
 
             @pl.when(inner)
@@ -397,13 +470,24 @@
 
         else:
             partial[owner] = through(0, hidden[0], owner).astype(jnp.bfloat16)
-        hand_out(partial, landed, owner, sum_send, sum_recv)
-
-    def guest_project(owner):
+        pl.when(is_last)(lambda: direct(partial, landed, owner, sum_send, sum_recv))
+        pl.when(both(other, jnp.logical_not(is_last)))(lambda: across(owner).start())
+
+    def guest_project(owner, is_last=None):
         @pl.when(helper)
         def _():
             guest_partial[owner] = through(1, guest_hidden, owner).astype(jnp.bfloat16)
-            hand_out(guest_partial, guest_landed, owner, guest_sum_send, guest_sum_recv)
+            def besides():
+                for k in range(1, pairs):
+                    beside(owner, k).start()
+
+            if is_last is None:
+                besides()
+            else:
+                pl.when(jnp.logical_not(is_last))(besides)
+                pl.when(is_last)(
+                    lambda: direct(guest_partial, guest_landed, owner, guest_direct, guest_sum_recv)
+                )
 
     def back(owner):
         return pltpu.make_async_remote_copy(
@@ -415,10 +499,10 @@
             device_id_type=MESH,
         )
 
-    def give_back(owner):
+    def give_back(owner, slots):
         @pl.when(helper)
         def _():
-            summed[owner] = gathered(guest_landed, owner, guest_sum_recv).astype(jnp.bfloat16)
+            summed[owner] = gathered(guest_landed, owner, slots, guest_sum_recv).astype(jnp.bfloat16)
             back(owner).start()
 
     scope = jax.named_scope
@@ -533,7 +617,10 @@
         with scope("b_near"):
             pieces_up(1, b_near)
 
-    nearer(*first)
+    with scope("a_first"):
+        each(*first, at_home)
+        for i in reversed(range(1, line - 1)):
+            each(*first, lambda which: arrive(which, owner_at(i)))
     if lent:
         others(lambda name, q: each(name, q, lambda which: own_line(which, False)))
 
@@ -547,28 +634,42 @@
             normalize(raw, normed)
 
     if lent:
+
+        def b_own():
+            groups(1, lambda name, q: up(1, name, q, normed, hidden[1]))
+
         with scope("b_far"):
             pieces_up(1, at_home)
             pieces_up(1, lambda which: arrive(which, last))
         with scope("b_own"):
-
-            @pl.when(inner)
-            def _():
-                groups(1, lambda name, q: up(1, name, q, normed, hidden[1]))
-    farthest(*first)
-    if lent:
+            pl.when(both(boss, inner))(b_own)
+
+        def c_early():
+            with scope("c_early"):
+                pieces_down(1, at_home)
+                pieces_down(1, lambda which: arrive_here(which, owner_at(1)))
+
+        pl.when(boss)(c_early)
         with scope("guest_wait"):
             pl.when(helper)(welcome)
+        pl.when(boss)(lambda: farthest(*first))
         with scope("b_guest"):
 
             @pl.when(helper)
             def _():
                 groups(1, lambda name, q: up(1, name, q, guest_normed, guest_hidden))
 
+    def early_folds():
+        def one(n, carry):
+            guest_fold(slice_at(n))
+            return carry
+
+        with scope("early_folds"):
+            lax.fori_loop(0, 2 * slices, one, 0)
+
     def guest_early():
         with scope("guest_early"):
-            pieces_down(1, at_home)
-            pieces_down(1, lambda which: arrive(which, owner_at(1)))
+            pieces_down(1, lambda which: pass_along(which, owner_at(1)))
 
             def early(j, carry):
                 guest_project(slice_at(j))
@@ -576,29 +677,45 @@
 
             lax.fori_loop(0, 2 * slices, early, 0)
 
+    if lent:
+        pl.when(other)(c_early)
+        pl.when(other)(guest_early)
     others(nearer)
     if lent:
-        guest_early()
+        pl.when(boss)(guest_early)
+        pl.when(other)(lambda: farthest(*first))
+    else:
+        farthest(*first)
+    if lent:
+        with scope("b_own"):
+            pl.when(both(other, inner))(b_own)
+        pl.when(other)(early_folds)
+
 
     def own_down(begin, stop):
         for r in range(begin, stop):
-            for kind in range(kinds):
+            for kind in reversed(range(kinds)):
                 own_line(piece("down", kind, 0, r), False)
 
     def own_up(name, q):
-        final = q == many[0] - 1 if not left_over[0] else here < (line if name == "rest" else 0)
-        pl.when(final)(lambda: own_down(0, 1))
+        if not lent:
+            final = q == many[0] - 1 if not left_over[0] else here < (line if name == "rest" else 0)
+            pl.when(final)(lambda: own_down(0, slices))
         if name == "wide" or many[0]:
             pl.when(jnp.logical_or(name == "rest", q > 0))(lambda: farthest(name, q))
-        pl.when(final)(lambda: own_down(1, slices))
         with scope("a_own"):
             up(0, name, q, normed, hidden[0])
 
     groups(0, own_up)
-
-    def collect(at):
+    with scope("c_near"):
+        pieces_down(0, lambda which: arrive(which, owner_at(1)))
+    if lent:
+        own_down(0, slices)
+        pl.when(boss)(early_folds)
+
+    def collect(at, slots):
         columns = pl.ds(pl.multiple_of(at * thin, thin), thin)
-        total = gathered(landed, at, sum_recv)
+        total = gathered(landed, at, slots, sum_recv)
 
         def keep(amount):
             out[:, columns] = (amount * gains[1:2, columns]).astype(jnp.bfloat16)
@@ -615,59 +732,106 @@
             keep(total)
 
     total_slices = line * slices
-    lag = min(2 * slices, total_slices)
-    late = max(slices - 1, 1)
+    near = 2 * slices
+
+    clip = lambda value, most: lax.clamp(0, value, most)
+
+    def own_folds(j):
+        return lax.min(
+            clip(2 * (j - near + 1), near) + clip(j - near - slices + 1, total_slices), folded
+        )
+
+    def collects(j):
+        return jnp.where(j < near + 2, 0, own_folds(j - 2))
+
+    def guest_folds(j):
+        late = jnp.where(j < near + slices, 1, 0)
+        return near + clip(j - near - late, folded - near)
+
+    def give_backs(j):
+        two_steps = lax.min(2 * (j - near + 1), guest_folds(j - 1))
+        return jnp.where(j < near, 0, two_steps + clip(j - folded, slices))
+
+    def advance(done, j, body, base=0):
+        def one(n, carry):
+            body(n)
+            return carry
+
+        lax.fori_loop(jnp.where(j > 0, done(j - 1), base), done(j), one, 0)
+
+    def complete(done, everything, body):
+        def one(n, carry):
+            body(n)
+            return carry
+
+        lax.fori_loop(done(jnp.int32(total_slices - 1)), everything, one, 0)
+
+    one_fold = lambda n: fold(slice_at(n))
+    one_collect = lambda n: collect(slice_at(n), pairs)
+    one_guest_fold = lambda n: guest_fold(slice_at(n))
+
+    def one_give_back(n):
+        pl.when(n < folded)(lambda: give_back(slice_at(n), parts))
+        pl.when(n >= folded)(lambda: give_back(slice_at(n), peers))
+
 
     def finish_line(j, carry):
-        i, r = j // slices, j % slices
-        owner = owner_at(i)
-        for kind in range(kinds):
+        p, r = j // slices, j % slices
+        owner = turn(p)
+        for kind in reversed(range(kinds)):
             which = piece("down", kind, 0, r)
             with scope(f"c_arrive#k={kind}"):
-                if kind:
-                    pl.when(i > 1)(lambda: arrive(which, owner))
-                else:
-                    pl.when(i == 0)(lambda: at_home(which))
-                    pl.when(i > 0)(lambda: arrive(which, owner))
+                if not kind:
+                    pl.when(p == 0)(lambda: at_home(which))
+                pl.when(p > 1)(lambda: arrive(which, owner))
+            if kind:
+                with scope("c_guest"):
+                    pl.when(p > 1)(lambda: guest_project(owner * slices + r, p == line - 1))
+        with scope("c_own"):
+            project(owner * slices + r, p == line - 1)
         if lent:
-            with scope("c_guest"):
-                pl.when(i > 1)(lambda: guest_project(owner * slices + r))
-            with scope("give_back"):
-                pl.when(i < 2)(lambda: give_back(slice_at(j)))
-        with scope("c_own"):
-            project(owner * slices + r)
+            with scope("guest_fold"):
+                advance(guest_folds, j, one_guest_fold, near)
+        with scope("fold"):
+            advance(own_folds, j, one_fold)
         if lent:
             with scope("give_back"):
-                pl.when(j >= 2 * slices + late)(lambda: give_back(slice_at(j - late)))
+                advance(give_backs, j, one_give_back)
         with scope("collect"):
-            pl.when(j >= lag)(lambda: collect(slice_at(j - lag)))
+            advance(collects, j, one_collect)
         return carry
 
     lax.fori_loop(0, total_slices, finish_line, 0)
-
     if lent:
-
-
-        def give_rest(j, carry):
-            with scope("give_rest"):
-                give_back(slice_at(j))
-            return carry
-
-        lax.fori_loop(total_slices - late, total_slices, give_rest, 0)
-
-    def rest_of_line(j, carry):
-        with scope("collect_rest"):
-            collect(slice_at(j))
+        with scope("guest_fold_rest"):
+            complete(guest_folds, folded, one_guest_fold)
+        with scope("give_rest"):
+            complete(give_backs, total_slices, one_give_back)
+    with scope("fold_rest"):
+        complete(own_folds, folded, one_fold)
+    with scope("collect_rest"):
+        complete(collects, folded, one_collect)
+
+    def collect_last(n, carry):
+        with scope("collect_last"):
+            collect(slice_at(n), peers)
         return carry
 
-    lax.fori_loop(total_slices - lag, total_slices, rest_of_line, 0)
+    lax.fori_loop(folded, total_slices, collect_last, 0)
 
     def departed(name, kind, amount, lane):
         part = store_rows(name, kind, pl.ds(0, amount * held))
         pltpu.make_async_copy(part, part, send_sem.at[stores[name, kind], lane]).wait()
 
     with scope("left"):
-        handed(landed, sum_send)
+        pl.when(boss)(lambda: handed(landed.at[:, pl.ds(0, peers - 1)], sum_send))
+
+        @pl.when(other)
+        def _():
+            handed(landed.at[pl.ds(0, slices)], sum_send)
+            if folded:
+                handed(x_stage.at[pl.ds(0, folded)], x_send)
+
 
         @pl.when(boss)
         def _():
@@ -693,7 +857,15 @@
                 pl.when(boss)(lambda: pass_across().wait_send())
                 for k in range(1, pairs):
                     pass_on(k).wait_send()
-                handed(guest_landed, guest_sum_send)
+                if pairs > 1:
+                    handed(y_stage.at[pl.ds(0, folded), pl.ds(0, pairs - 1)], y_send)
+
+                def guests_left(in_two, at_once):
+                    handed(guest_landed.at[pl.ds(0, folded), pl.ds(0, in_two)], guest_sum_send)
+                    handed(guest_landed.at[pl.ds(0, slices), pl.ds(0, at_once)], guest_direct)
+
+                pl.when(boss)(lambda: guests_left(parts - 1, peers - 1))
+                pl.when(other)(lambda: guests_left(parts, peers))
                 pltpu.make_async_copy(summed, summed, back_send).wait()
 
 
@@ -729,11 +901,14 @@
             pltpu.VMEM((2, width), full),
             pltpu.VMEM((line * slices, rows, thin), half),
             pltpu.VMEM((line * slices, peers, kept, thin), half),
+            pltpu.VMEM((line * slices, rows, thin), half),
             dma((3 * len(spans), 3)),
             dma((pieces, line)),
             dma((2 * len(spans) + 2,)),
             dma((4,)),
             dma((2,)),
+            dma,
+            dma((line * slices,)),
             dma,
             dma((line * slices,)),
         ]
@@ -744,6 +919,7 @@
                 pltpu.VMEM((rows, lent), half),
                 pltpu.VMEM((line * slices, rows, thin), half),
                 pltpu.VMEM((line * slices, peers, kept, thin), half),
+                pltpu.VMEM((line * slices, pairs, parts * kept, thin), half),
                 pltpu.VMEM((line * slices, kept, thin), half),
                 pltpu.VMEM((line * slices, kept, thin), half),
                 dma((pairs + 1,)),
@@ -751,11 +927,14 @@
                 dma,
                 dma((line * slices,)),
                 dma,
+                dma,
+                dma((line * slices,)),
+                dma,
                 dma((line * slices,)),
             ]
         return pl.pallas_call(
             functools.partial(kernel, parts, line, peers, lent, slices),
-            out_shape=jax.ShapeDtypeStruct((kept, width), half),
+            out_shape=pltpu.VMEM((kept, width), half),
             in_specs=[
                 pl.BlockSpec(memory_space=pl.ANY if i in (0, 2, 3, 4) else pltpu.VMEM)
                 for i in range(12)

time: 118 us -> 115 us (0.975)
  Pallas kernels: 116 us -> 114 us
    pallas_call x1, Pallas kernels: 116 us -> 114 us  [local(): pl.pallas_call(functools.partial(kernel, parts, line, peers, lent, slices...]
where the time goes in v3:
time: 115 us
  Pallas kernels  114 us (99%)
    pallas_call x1, Pallas kernels, local(): pl.pallas_call(functools.partial(kernel, parts, line, peers, lent, slices...  114 us

profile of v3, /device:TPU:0, one launch (start us, length us, event | category | flops | bytes accessed | tf_op | source)
XLA Modules:
  0.0 114.8 jit_solution(14502984066870653059)
XLA Ops:
  0.0 114.0 %shard_map.118 = bf16[128,2048]{1,0:T(8,128)(2,1)S(1)} custom-call(bf16[512,2048]{1,0:T(8,128)(2,1)} %tokens.1, f32[2048]{0:T(1024)} %norm_gain.1, f32[512,1408]{1,0:T(8,128)} %value_weight.1, f32[512,1408]{1,0:T(8,128)} %gate_weight.1, f32[512,1408]{1,0:T(8,128)} %down_weight.1, f32[1408]{0:T(1024)} %value_scale.1, f32[1408]{0:T(1024)} %gate_scale.1, ...), custom_call_target="tpu_custom_call" | custom-call | tf_op jit(solution)/shard_map/pallas_call | solution.py:935
  114.0 0.8 copy.14

commit v4 on v3

--- a/solution.py
+++ b/solution.py
@@ -737,20 +737,18 @@
     clip = lambda value, most: lax.clamp(0, value, most)
 
     def own_folds(j):
-        return lax.min(
-            clip(2 * (j - near + 1), near) + clip(j - near - slices + 1, total_slices), folded
-        )
+        early = clip(2 * (j - near + 1), near)
+        later = clip(2 * (j - near - slices + 1), total_slices)
+        return lax.min(lax.min(early + later, folded), lax.max(j, 0))
 
     def collects(j):
         return jnp.where(j < near + 2, 0, own_folds(j - 2))
 
     def guest_folds(j):
-        late = jnp.where(j < near + slices, 1, 0)
-        return near + clip(j - near - late, folded - near)
+        return near + clip(j - near - 1, folded - near)
 
     def give_backs(j):
-        two_steps = lax.min(2 * (j - near + 1), guest_folds(j - 1))
-        return jnp.where(j < near, 0, two_steps + clip(j - folded, slices))
+        return jnp.where(j < near, 0, lax.min(2 * (j - near + 1), guest_folds(j - 2)))
 
     def advance(done, j, body, base=0):
         def one(n, carry):

time: 115 us -> 113 us (0.983)
  Pallas kernels: 114 us -> 112 us
    pallas_call x1, Pallas kernels: 114 us -> 112 us  [local(): pl.pallas_call(functools.partial(kernel, parts, line, peers, lent, slices...]
where the time goes in v4:
time: 113 us
  Pallas kernels  112 us (99%)
    pallas_call x1, Pallas kernels, local(): pl.pallas_call(functools.partial(kernel, parts, line, peers, lent, slices...  112 us

profile of v4, /device:TPU:0, one launch (start us, length us, event | category | flops | bytes accessed | tf_op | source)
XLA Modules:
  0.0 113.0 jit_solution(9424397764768662866)
XLA Ops:
  0.0 112.2 %shard_map.118 = bf16[128,2048]{1,0:T(8,128)(2,1)S(1)} custom-call(bf16[512,2048]{1,0:T(8,128)(2,1)} %tokens.1, f32[2048]{0:T(1024)} %norm_gain.1, f32[512,1408]{1,0:T(8,128)} %value_weight.1, f32[512,1408]{1,0:T(8,128)} %gate_weight.1, f32[512,1408]{1,0:T(8,128)} %down_weight.1, f32[1408]{0:T(1024)} %value_scale.1, f32[1408]{0:T(1024)} %gate_scale.1, ...), custom_call_target="tpu_custom_call" | custom-call | tf_op jit(solution)/shard_map/pallas_call | solution.py:933
  112.2 0.8 copy.14
